TPU v7x, 128 devices: a whole 4x4x4 slice. The times are simulated.
128 devices in a mesh: sp: 16 (over z, x), dp: 8 (over y, core).
Axes of the slice: x: 4, y: 4, z: 4, core: 2. Of those that a mesh axis runs over, the one named last changes fastest.
Arguments:
- residual: bfloat16 [8, 2048, 2048], P('dp', 'sp'), may hold values from -6 to 6
- query_projected: bfloat16 [8, 2048, 1024], P('dp', 'sp'), may hold values from -6 to 6
- key_projected: bfloat16 [8, 2048, 1024], P('dp', 'sp'), may hold values from -6 to 6
- value_projected: bfloat16 [8, 2048, 1024], P('dp', 'sp'), may hold values from -6 to 6
- output_gate_proj: bfloat16 [8, 2048, 1024], P('dp', 'sp'), may hold values from -6 to 6
- write_strength_logits: float32 [8, 2048, 16], P('dp', 'sp'), may hold values from -6 to 6
- decay_logits: float32 [8, 2048, 16], P('dp', 'sp'), may hold values from -5 to 5
- extra_log_decay: float32 [8, 2048, 16], P('dp', 'sp'), may hold values from -0.7 to 0
- head_decay_rate: float32 [16], P('sp'), may hold values from 0 to 0.06
- head_norm_gain: float32 [64], replicated, may hold values from 0.1 to 1.9
- output_matrix: bfloat16 [1024, 2048], replicated, may hold values from -0.1875 to 0.1875
- expert_norm_gain: float32 [2048], replicated, may hold values from 0.1 to 1.9
- group_router_scores: float32 [8, 2048, 4], P('dp', 'sp'), may hold values from -6 to 6
- chosen_expert_scores: float32 [8, 2048, 2], P('dp', 'sp'), may hold values from -6 to 6
- routes: int32 [8, 2048, 2], P('dp', 'sp'), may hold values from 0 to 127, as said below
- gate_weight: bfloat16 [128, 2048, 1024], P(('sp', 'dp')), may hold values from -0.125 to 0.125
- up_weight: bfloat16 [128, 2048, 1024], P(('sp', 'dp')), may hold values from -0.125 to 0.125
- down_weight: bfloat16 [128, 1024, 2048], P(('sp', 'dp')), may hold values from -0.75 to 0.75
Outputs:
- layer_out: bfloat16 [8, 2048, 2048], P('dp', 'sp')
Inputs may be any that keep to these rules, and one draw needn't show every extreme that they name: `routes`: the 2 numbers of a row differ and lie in one group of 32 consecutive experts. Among the rows of one device no expert is named more than 4 times, some expert exactly 4 times, and each group is named by exactly 32 rows.
All inputs are finite; a program needn't handle non-finite values.
Results may differ from a plain program's by a relative error of at most 0.0059.
Values may be sent and summed in bfloat16 or wider, within the bound.
A program may use at most 128 MiB of HBM per device.

v0:
```python
import jax
import jax.numpy as jnp
from jax import lax
from jax.sharding import Mesh
from jax.sharding import PartitionSpec as P

BLK = 64
SP = ("sp_0", "sp_1")
SP_DP = ("sp_0", "sp_1", "dp")


eps = 1e-06


def sent_together(arrays, axis, split_dim, concat_dim, along):
    both = jnp.concatenate(arrays, axis=along)
    result, at, done = (
        lax.all_to_all(both, axis, split_axis=split_dim, concat_axis=concat_dim, tiled=True),
        0,
        [],
    )
    for a in arrays:
        done.append(lax.slice_in_dim(result, at, at + a.shape[along], axis=along))
        at += a.shape[along]
    return tuple(done)


def in_blocks(array, dim, count):
    before, after = (array.shape[:dim], array.shape[dim + 1 :])
    return jnp.moveaxis(array.reshape(*before, count, -1, *after), dim, 0)


def laid_out(parts, dim):
    parts = jnp.moveaxis(parts, 0, dim)
    lengths = parts.shape
    return parts.reshape(*lengths[:dim], lengths[dim] * lengths[dim + 1], *lengths[dim + 2 :])


def turned_blocks(parts, axes, sequence):
    inside = parts.shape[1:]
    result = parts.reshape(*(lax.axis_size(a) for a in axes), *inside)
    for k in sequence:
        result = lax.all_to_all(result, axes[k], k, k, tiled=True)
    return result.reshape(-1, *inside)


def one_axis_at_a_time(array, axes, sequence, split_dim, concat_dim):
    parts = in_blocks(array, split_dim, lax.axis_size(axes))
    return laid_out(turned_blocks(parts, axes, sequence), concat_dim)


def one_exchange(array, axis, axes, splits, concats):
    sizes = [lax.axis_size(a) for a in axes]
    parts = in_blocks(array, splits[0], sizes[0])
    parts = jnp.moveaxis(in_blocks(parts, splits[1] + 1, sizes[1]), 0, 1)
    inside = parts.shape[2:]
    parts = parts.reshape(-1, *inside)
    parts = lax.all_to_all(parts, axis, split_axis=0, concat_axis=0, tiled=True)
    parts = laid_out(parts.reshape(*sizes, *inside), concats[0] + 1)
    return laid_out(parts, concats[1])


def unit_rows(array):
    return array * lax.rsqrt(jnp.sum(array * array, axis=-1, keepdims=True) + eps)


def block_terms(query, keyed, valued, beta, log_decay_total, span):
    length, width = query.shape
    count = length // span
    highest_precision = lax.Precision.HIGHEST
    qb = query.reshape(count, span, width)
    kb = keyed.reshape(count, span, width)
    vb = valued.reshape(count, span, width)
    bb = beta.reshape(count, span)
    cumul = jnp.cumsum(log_decay_total.reshape(count, span), axis=1)
    rows = jnp.arange(span, dtype=jnp.int32)
    causal = rows[:, None] >= rows[None, :]
    strict = rows[:, None] > rows[None, :]
    diff = cumul[:, :, None] - cumul[:, None, :]
    decay = jnp.where(causal, jnp.exp(jnp.where(causal, diff, 0.0)), 0.0)
    kbeta = kb * bb[..., None]
    lower = jnp.where(
        strict, jnp.einsum("nid,njd->nij", kbeta, kb, precision=highest_precision) * decay, 0.0
    )
    rhs = jnp.concatenate([vb * bb[..., None], kbeta * jnp.exp(cumul)[..., None]], axis=-1)
    solved = jax.scipy.linalg.solve_triangular(lower, rhs, lower=True, unit_diagonal=True)
    state_update = solved[..., :width]
    write_decayed = solved[..., width:]
    attention_out = jnp.einsum("nid,njd->nij", qb, kb, precision=highest_precision) * decay
    query_decayed = qb * jnp.exp(cumul)[..., None]
    key_decayed = kb * jnp.exp(cumul[:, -1:] - cumul)[..., None]
    total = jnp.exp(cumul[:, -1])
    return (attention_out, query_decayed, write_decayed, state_update, key_decayed, total)


def compose(earlier, later):
    highest_precision = lax.Precision.HIGHEST
    first_map, first_add = earlier
    second_map, second_add = later
    joined_map = jnp.einsum("nij,njk->nik", second_map, first_map, precision=highest_precision)
    joined_add = (
        jnp.einsum("nij,njk->nik", second_map, first_add, precision=highest_precision) + second_add
    )
    return (joined_map, joined_add)


def run_head(query, keyed, valued, beta, log_decay_total):
    length, width = query.shape
    highest_precision = lax.Precision.HIGHEST
    attention_out, query_decayed, write_decayed, state_update, key_decayed, total = block_terms(
        query, keyed, valued, beta, log_decay_total, BLK
    )
    identity = jnp.eye(width, dtype=jnp.float32)
    carry_map = total[:, None, None] * identity - jnp.einsum(
        "ulc,ulq->ucq", key_decayed, write_decayed, precision=highest_precision
    )
    carry_combine = jnp.einsum(
        "ulc,ulq->ucq", key_decayed, state_update, precision=highest_precision
    )
    _, reached = lax.associative_scan(compose, (carry_map, carry_combine))
    start_offsets = jnp.concatenate(
        [jnp.zeros((1, width, width), jnp.float32), reached[:-1]], axis=0
    )
    value_corrected = state_update - jnp.einsum(
        "pzg,pgj->pzj", write_decayed, start_offsets, precision=highest_precision
    )
    final_output = jnp.einsum(
        "pzg,pgj->pzj", query_decayed, start_offsets, precision=highest_precision
    ) + jnp.einsum("xyr,xrt->xyt", attention_out, value_corrected, precision=highest_precision)
    return final_output.reshape(length, width)


def expert_apply(arrived, gate_weight, up_weight, down_weight):
    width = arrived.shape[-1]
    rows = arrived.reshape(-1, width)
    gate = jnp.dot(rows, gate_weight[0], preferred_element_type=jnp.float32)
    upper = jnp.dot(rows, up_weight[0], preferred_element_type=jnp.float32)
    hidden = (jax.nn.silu(gate) * upper).astype(jnp.bfloat16)
    final_output = jnp.dot(hidden, down_weight[0], preferred_element_type=jnp.float32).astype(
        jnp.bfloat16
    )
    return final_output.reshape(arrived.shape)


def shards(
    residual,
    query_projected,
    key_projected,
    value_projected,
    output_gate_proj,
    write_strength_logits,
    decay_logits,
    extra_log_decay,
    head_decay_rate,
    head_norm_gain,
    output_matrix,
    expert_norm_gain,
    group_router_scores,
    chosen_expert_scores,
    routes,
    gate_weight,
    up_weight,
    down_weight,
):
    q_heads, k_heads, v_heads = sent_together(
        (query_projected, key_projected, value_projected), SP, 2, 1, 0
    )
    b_heads, d_heads, u_heads = sent_together(
        (write_strength_logits, decay_logits, extra_log_decay), SP, 2, 1, 0
    )
    seqs, length, local = q_heads.shape
    heads_here = head_decay_rate.shape[0]
    width = local // heads_here

    def heads_of(array):
        return (
            array.astype(jnp.float32)
            .reshape(seqs, length, heads_here, width)
            .transpose(0, 2, 1, 3)
            .reshape(seqs * heads_here, length, width)
        )

    query = unit_rows(heads_of(q_heads)) * width ** (-0.5)
    keyed = unit_rows(heads_of(k_heads))
    valued = heads_of(v_heads)
    beta = jax.nn.sigmoid(b_heads).transpose(0, 2, 1).reshape(seqs * heads_here, length)
    log_decay_total = -head_decay_rate[None, :, None] * jax.nn.softplus(
        d_heads.transpose(0, 2, 1)
    ) + u_heads.transpose(0, 2, 1)
    log_decay_total = log_decay_total.reshape(seqs * heads_here, length)
    attended = jax.vmap(run_head)(query, keyed, valued, beta, log_decay_total)
    normed = (
        attended
        * lax.rsqrt(jnp.mean(attended * attended, axis=-1, keepdims=True) + eps)
        * head_norm_gain
    )
    normed = (
        normed.astype(jnp.bfloat16)
        .reshape(seqs, heads_here, length, width)
        .transpose(0, 2, 1, 3)
        .reshape(seqs, length, local)
    )
    returned = one_axis_at_a_time(normed, SP, (0, 1), 1, 2)
    tok_rows = residual.shape[1]
    model = residual.shape[2]
    gated = (
        returned[0].astype(jnp.float32) * jax.nn.silu(output_gate_proj[0].astype(jnp.float32))
    ).astype(jnp.bfloat16)
    mixed = residual[0].astype(jnp.float32) + jnp.dot(
        gated, output_matrix, preferred_element_type=jnp.float32
    )
    ffn_in = (
        mixed * lax.rsqrt(jnp.mean(mixed * mixed, axis=-1, keepdims=True) + eps) * expert_norm_gain
    ).astype(jnp.bfloat16)
    sp_count = lax.axis_size(SP)
    dp_count = lax.axis_size("dp")
    experts = sp_count * dp_count
    groups = group_router_scores.shape[-1]
    per_group = experts // groups
    capacity = 4 * tok_rows // experts
    chosen = routes[0]
    flat = chosen.reshape(-1)
    onehot = (flat[:, None] == jnp.arange(experts, dtype=jnp.int32)[None, :]).astype(jnp.int32)
    rank = jnp.sum((jnp.cumsum(onehot, axis=0) - onehot) * onehot, axis=1)
    slot = flat * capacity + rank
    owners = jnp.arange(2 * tok_rows, dtype=jnp.int32) // 2
    slot_tok = jnp.full((experts * capacity,), tok_rows, jnp.int32).at[slot].set(owners)
    outgoing = jnp.take(ffn_in, slot_tok, axis=0, mode="fill", fill_value=0).reshape(
        experts, capacity, model
    )
    outgoing_grid = outgoing.reshape(sp_count, dp_count, capacity, model)
    arrived = one_exchange(outgoing_grid, SP_DP, (SP, "dp"), (0, 1), (0, 1))
    produced = expert_apply(arrived, gate_weight, up_weight, down_weight)
    came_back = one_exchange(produced, SP_DP, (SP, "dp"), (0, 1), (0, 1))
    back_rows = came_back.reshape(experts * capacity, model)
    picked = jnp.take(back_rows, slot, axis=0).reshape(tok_rows, 2, model)
    group_exp = jnp.exp(group_router_scores[0])
    group_id = chosen[:, 0] // per_group
    match = jnp.arange(groups, dtype=jnp.int32)[None, :] == group_id[:, None]
    group_prob = jnp.sum(jnp.where(match, group_exp, 0.0), axis=-1) / jnp.sum(group_exp, axis=-1)
    pick_exp = jnp.exp(chosen_expert_scores[0])
    weight = group_prob[:, None] * pick_exp / jnp.sum(pick_exp, axis=-1, keepdims=True)
    moe = jnp.sum(weight[..., None] * picked.astype(jnp.float32), axis=1)
    return (mixed + moe).astype(jnp.bfloat16)[None]


def solution(mesh):
    split = Mesh(mesh.devices.reshape(4, 4, mesh.shape["dp"]), ("sp_0", "sp_1", "dp"))
    in_specs = (
        P("dp", SP, None),
        P("dp", SP, None),
        P("dp", SP, None),
        P("dp", SP, None),
        P("dp", SP, None),
        P("dp", SP, None),
        P("dp", SP, None),
        P("dp", SP, None),
        P(SP),
        P(),
        P(),
        P(),
        P("dp", SP, None),
        P("dp", SP, None),
        P("dp", SP, None),
        P(SP_DP, None, None),
        P(SP_DP, None, None),
        P(SP_DP, None, None),
    )
    out_specs = P("dp", SP, None)
    return jax.shard_map(
        shards, mesh=split, in_specs=in_specs, out_specs=out_specs, check_vma=False
    )
```

profile of v0, /device:TPU:1, one launch (start us, length us, event | category | flops | bytes accessed | tf_op | source)
XLA Modules:
  0.0 327.6 jit_solution(17115278893464206473)
XLA Ops:
  1.4 8.4 %all-to-all-start.1 = ((f32[3,128,16]{1,0,2:T(4,128)}), f32[3,128,16]{1,0,2:T(4,128)S(1)}, u32[]{:S(2)}, u32[]{:S(2)}) async-start(f32[3,128,16]{1,0,2:T(4,128)} %copy.173), calls=%async_computation.1 | async-start | bytes 65536 | tf_op jit(solution)/shard_map/all_to_all | solution.py:18
  15.5 2.8 pad_maximum_fusion
  20.4 7.1 %all-to-all-start = ((bf16[3,128,1024]{1,0,2:T(4,128)(2,1)}), bf16[3,128,1024]{1,0,2:T(4,128)(2,1)S(1)}, u32[]{:S(2)}, u32[]{:S(2)}) async-start(bf16[3,128,1024]{1,0,2:T(4,128)(2,1)} %pad_maximum_fusion), calls=%async_computation | async-start | bytes 2097152 | tf_op jit(solution)/shard_map/all_to_all | solution.py:18
  28.4 14.6 %all-to-all-done = bf16[3,128,1024]{1,0,2:T(4,128)(2,1)S(1)} async-done(((bf16[3,128,1024]{1,0,2:T(4,128)(2,1)}), bf16[3,128,1024]{1,0,2:T(4,128)(2,1)S(1)}, u32[]{:S(2)}, u32[]{:S(2)}) %all-to-all-start) | async-done | bytes 786464 | tf_op jit(solution)/shard_map/all_to_all | solution.py:18
  60.7 7.5 %fusion.9 = (f32[32,64,64]{0,2,1:T(8,128)}, f32[1,32,1,64,64]{1,4,3,2,0:T(8,128)}) fusion(f32[32,64,64]{0,2,1:T(8,128)} %copy.190, f32[32,64]{0,1:T(8,128)S(1)} %copy.178, pred[64,64]{1,0:T(8,128)(4,1)S(1)} %get-tuple-element.30, f32[64,64]{1,0:T(8,128)S(1)} %get-tuple-element.33, f32[32,64,64]{0,2,1:T(8,128)} %copy.180, ...), kind=kLoop, calls=%fused_computation.16 | loop fusion | flops 1048576 | bytes 2134016 | tf_op jit(solution)/shard_map/vmap()/mul | solution.py:89
  68.1 68.4 %custom-call.4 = f32[1,32,1,64,64]{1,3,4,2,0:T(8,128)} custom-call(f32[1,32,1,64,64]{1,4,3,2,0:T(8,128)} %get-tuple-element.15), custom_call_target="InvertDiagBlocksLowerTriangular" | custom-call | tf_op jit(solution)/shard_map/vmap(jit(_solve_triangular))/vmap()/triangular_solve | solution.py:86
  136.5 3.0 copy.183
  160.3 6.2 %pad.99 = f32[1,32,64,64]{3,2,1,0:T(8,128)S(1)} pad(f32[1,16,64,64]{3,2,1,0:T(8,128)} %add.226, f32[]{:T(128)} %constant.82.clone.1), padding=0_0_0x1_0_1x0_0_0x0_0_0 | pad | bytes 786436
  168.4 6.4 %pad.61 = f32[1,31,64,64]{3,2,1,0:T(8,128)S(1)} pad(f32[1,16,64,64]{3,2,1,0:T(8,128)} %pad_maximum_fusion.1, f32[]{:T(128)} %constant.82.clone.1), padding=0_0_0x0_0_1x0_0_0x0_0_0 | pad | bytes 770052 | tf_op jit(solution)/shard_map/vmap()/slice | solution.py:122
  176.2 3.3 %fusion.27 = f32[32,64,64]{1,2,0:T(8,128)} fusion(f32[32,64,64]{1,0,2:T(8,128)S(1)} %copy-done.3, f32[1,31,64,64]{3,2,1,0:T(8,128)S(1)} %slice_add_fusion), kind=kOutput, calls=%fused_computation.54 | convolution fusion | flops 100663296 | bytes 1556480 | tf_op jit(solution)/shard_map/vmap(pzg,pgj->pzj)/dot_general | solution.py:127
  181.3 3.4 %multiply_reduce_fusion.2 = (f32[32,64]{1,0:T(8,128)S(1)}, f32[32,64,64]{1,2,0:T(8,128)S(1)}) fusion(f32[32,64,64]{1,2,0:T(8,128)} %fusion.27, f32[32,64,64]{2,1,0:T(8,128)} %copy.191, f32[32,64,64]{2,1,0:T(8,128)S(1)} %fusion.14), kind=kOutput, calls=%fused_computation.65 | convolution fusion | flops 101054464 | bytes 2105344 | tf_op jit(solution)/shard_map/vmap(xyr,xrt->xyt)/dot_general | solution.py:129
  186.7 3.4 %all-to-all-start.2 = ((bf16[4,4,1,128,64]{3,1,4,2,0:T(4,128)(2,1)}), bf16[4,4,1,128,64]{3,1,4,2,0:T(4,128)(2,1)S(1)}, u32[]{:S(2)}, u32[]{:S(2)}) async-start(bf16[4,4,1,128,64]{3,1,4,2,0:T(4,128)(2,1)} %copy.194), calls=%async_computation.2 | async-start | bytes 524288 | tf_op jit(solution)/shard_map/all_to_all | solution.py:43
  190.1 5.5 %all-to-all-done.2 = bf16[4,4,1,128,64]{3,1,4,2,0:T(4,128)(2,1)S(1)} async-done(((bf16[4,4,1,128,64]{3,1,4,2,0:T(4,128)(2,1)}), bf16[4,4,1,128,64]{3,1,4,2,0:T(4,128)(2,1)S(1)}, u32[]{:S(2)}, u32[]{:S(2)}) %all-to-all-start.2) | async-done | bytes 262176 | tf_op jit(solution)/shard_map/all_to_all | solution.py:43
  196.5 3.5 %all-to-all-start.3 = ((bf16[4,4,1,128,64]{3,0,4,2,1:T(4,128)(2,1)}), bf16[4,4,1,128,64]{3,0,4,2,1:T(4,128)(2,1)S(1)}, u32[]{:S(2)}, u32[]{:S(2)}) async-start(bf16[4,4,1,128,64]{3,0,4,2,1:T(4,128)(2,1)} %copy.195), calls=%async_computation.3 | async-start | bytes 524288 | tf_op jit(solution)/shard_map/all_to_all | solution.py:43
  200.3 5.2 %all-to-all-done.3 = bf16[4,4,1,128,64]{3,0,4,2,1:T(4,128)(2,1)S(1)} async-done(((bf16[4,4,1,128,64]{3,0,4,2,1:T(4,128)(2,1)}), bf16[4,4,1,128,64]{3,0,4,2,1:T(4,128)(2,1)S(1)}, u32[]{:S(2)}, u32[]{:S(2)}) %all-to-all-start.3) | async-done | bytes 262176 | tf_op jit(solution)/shard_map/all_to_all | solution.py:43
  205.7 3.0 multiply_reduce_fusion.1
  208.9 3.3 %gather_fusion = bf16[512,2048]{1,0:T(8,128)(2,1)} fusion(bf16[128,2048]{1,0:T(8,128)(2,1)S(1)} %multiply_convert_fusion.1, s32[1024]{0:T(1024)S(1)} %pad_clamp_fusion.1), kind=kCustom, calls=%fused_computation | custom fusion | bytes 4196352 | tf_op jit(solution)/shard_map/jit(_take)/gather | solution.py:228
  216.0 40.4 %all_to_all.50 = bf16[128,1,1,4,2048]{4,3,2,1,0:T(4,128)(2,1)S(1)} all-to-all(bf16[128,1,1,4,2048]{4,3,2,1,0:T(4,128)(2,1)S(1)} %bitcast_select_fusion), channel_id=1, replica_groups=mesh['sp_0'=4,'sp_1'=4,'dp'=8] {'sp_0','sp_1','dp'}, dimensions={0} | all-to-all | bytes 4194304 | tf_op jit(solution)/shard_map/all_to_all | solution.py:58
  258.4 6.6 %fusion.4 = f32[512,1024]{1,0:T(8,128)} fusion(bf16[512,2048]{1,0:T(8,128)(2,1)} %reshape_reshape.7, bf16[1,2048,1024]{2,1,0:T(8,128)(2,1)} %param.33), kind=kOutput, calls=%fused_computation.7 | convolution fusion | flops 2147483648 | bytes 8388608 | tf_op jit(solution)/shard_map/dot_general | solution.py:136
  265.1 9.9 %fusion.6 = bf16[512,2048]{1,0:T(8,128)(2,1)} fusion(bf16[1,1024,2048]{2,1,0:T(8,128)(2,1)} %param.35, f32[512,1024]{1,0:T(8,128)} %fusion.4, bf16[512,2048]{1,0:T(8,128)(2,1)S(1)} %copy-done.6, bf16[1,2048,1024]{2,1,0:T(8,128)(2,1)} %param.34), kind=kOutput, calls=%fused_computation.9 | convolution fusion | flops 4299161600 | bytes 14680064 | tf_op jit(solution)/shard_map/dot_general | solution.py:139
  275.0 4.1 %reshape_transpose_transpose_reshape_reshape_reshape.3 = bf16[128,1,1,4,2048]{4,3,0,2,1:T(4,128)(2,1)} reshape(bf16[512,2048]{1,0:T(8,128)(2,1)} %fusion.6) | data formatting | bytes 4194304 | tf_op jit(solution)/shard_map/reshape;transpose;transpose;reshape;reshape;reshape | solution.py:57
  279.1 4.9 %all-to-all-start.5 = ((bf16[128,1,1,4,2048]{4,3,2,1,0:T(4,128)(2,1)}), bf16[128,1,1,4,2048]{4,3,2,1,0:T(4,128)(2,1)S(1)}, u32[]{:S(2)}, u32[]{:S(2)}) async-start(bf16[128,1,1,4,2048]{4,3,2,1,0:T(4,128)(2,1)} %bitcast.277), calls=%async_computation.5 | async-start | bytes 4194304 | tf_op jit(solution)/shard_map/all_to_all | solution.py:58
  284.6 29.6 %all-to-all-done.5 = bf16[128,1,1,4,2048]{4,3,2,1,0:T(4,128)(2,1)S(1)} async-done(((bf16[128,1,1,4,2048]{4,3,2,1,0:T(4,128)(2,1)}), bf16[128,1,1,4,2048]{4,3,2,1,0:T(4,128)(2,1)S(1)}, u32[]{:S(2)}, u32[]{:S(2)}) %all-to-all-start.5) | async-done | bytes 2097184 | tf_op jit(solution)/shard_map/all_to_all | solution.py:58
  322.2 4.1 %multiply_reduce_fusion = f32[128,2048]{1,0:T(8,128)S(1)} fusion(bf16[128,2,2048]{2,1,0:T(2,128)(2,1)S(1)} %gather.15, pred[128,2]{1,0:T(8,128)(4,1)S(1)} %copy.204, f32[128,2]{1,0:T(8,128)S(1)} %copy.198), kind=kLoop, calls=%fused_computation.12 | loop fusion | flops 1835008 | bytes 2098432 | tf_op jit(solution)/shard_map/reduce_sum | solution.py:243
  (165 shorter events, 71.1 us)
Async XLA Ops:
  0.0 14.2 %copy-start.8 = (bf16[1,128,1024]{2,1,0:T(8,128)(2,1)S(1)}, bf16[1,128,1024]{2,1,0:T(8,128)(2,1)}, u32[]{:S(2)}) copy-start(bf16[1,128,1024]{2,1,0:T(8,128)(2,1)} %param.21) | copy-start | bytes 786436
  1.4 19.0 %all-to-all-start.1 = ((f32[3,128,16]{1,0,2:T(4,128)}), f32[3,128,16]{1,0,2:T(4,128)S(1)}, u32[]{:S(2)}, u32[]{:S(2)}) async-start(f32[3,128,16]{1,0,2:T(4,128)} %copy.173), calls=%async_computation.1 | async-start | bytes 65536 | tf_op jit(solution)/shard_map/all_to_all | solution.py:18
  20.4 22.6 %all-to-all-start = ((bf16[3,128,1024]{1,0,2:T(4,128)(2,1)}), bf16[3,128,1024]{1,0,2:T(4,128)(2,1)S(1)}, u32[]{:S(2)}, u32[]{:S(2)}) async-start(bf16[3,128,1024]{1,0,2:T(4,128)(2,1)} %pad_maximum_fusion), calls=%async_computation | async-start | bytes 2097152 | tf_op jit(solution)/shard_map/all_to_all | solution.py:18
  136.5 5.4 %copy-start.4 = (f32[1,16,128,64]{3,2,1,0:T(8,128)S(1)}, f32[1,16,128,64]{3,2,1,0:T(8,128)}, u32[]{:S(2)}) copy-start(f32[1,16,128,64]{3,2,1,0:T(8,128)} %copy.182) | copy-start | bytes 1572868
  147.2 2.4 copy-start.2
  150.3 0.8 copy-start.5
  152.9 3.9 %slice-start.1 = ((f32[1,16,64,64]{3,2,1,0:T(8,128)}), f32[1,1,64,64]{3,2,1,0:T(8,128)S(1)}, s32[]{:S(2)}) async-start(f32[1,16,64,64]{3,2,1,0:T(8,128)} %copy-done.5), calls=%async_computation.7 | async-start | bytes 65536 | tf_op jit(solution)/shard_map/vmap()/slice | solution.py:120
  157.9 8.6 %slice-start = ((f32[1,32,64,64]{3,2,1,0:T(8,128)}), f32[1,1,64,64]{3,2,1,0:T(8,128)S(1)}, s32[]{:S(2)}) async-start(f32[1,32,64,64]{3,2,1,0:T(8,128)} %copy-done.2), calls=%async_computation.6 | async-start | bytes 65536 | tf_op jit(solution)/shard_map/vmap()/slice | solution.py:120
  174.9 1.3 copy-start.3
  176.2 3.3 %copy-start = (f32[32,64,64]{0,2,1:T(8,128)S(1)}, f32[32,64,64]{0,2,1:T(8,128)}, u32[]{:S(2)}) copy-start(f32[32,64,64]{0,2,1:T(8,128)} %get-tuple-element.14) | copy-start | bytes 1572868
  184.7 1.0 copy-start.14
  185.3 14.7 %copy-start.9 = (bf16[1,128,1024]{2,1,0:T(8,128)(2,1)S(1)}, bf16[1,128,1024]{2,1,0:T(8,128)(2,1)}, u32[]{:S(2)}) copy-start(bf16[1,128,1024]{2,1,0:T(8,128)(2,1)} %param.22) | copy-start | bytes 786436
  185.9 19.8 %copy-start.7 = (bf16[1,128,2048]{2,1,0:T(8,128)(2,1)S(1)}, bf16[1,128,2048]{2,1,0:T(8,128)(2,1)}, u32[]{:S(2)}) copy-start(bf16[1,128,2048]{2,1,0:T(8,128)(2,1)} %param.18) | copy-start | bytes 1572868
  186.7 8.9 %all-to-all-start.2 = ((bf16[4,4,1,128,64]{3,1,4,2,0:T(4,128)(2,1)}), bf16[4,4,1,128,64]{3,1,4,2,0:T(4,128)(2,1)S(1)}, u32[]{:S(2)}, u32[]{:S(2)}) async-start(bf16[4,4,1,128,64]{3,1,4,2,0:T(4,128)(2,1)} %copy.194), calls=%async_computation.2 | async-start | bytes 524288 | tf_op jit(solution)/shard_map/all_to_all | solution.py:43
  196.5 9.0 %all-to-all-start.3 = ((bf16[4,4,1,128,64]{3,0,4,2,1:T(4,128)(2,1)}), bf16[4,4,1,128,64]{3,0,4,2,1:T(4,128)(2,1)S(1)}, u32[]{:S(2)}, u32[]{:S(2)}) async-start(bf16[4,4,1,128,64]{3,0,4,2,1:T(4,128)(2,1)} %copy.195), calls=%async_computation.3 | async-start | bytes 524288 | tf_op jit(solution)/shard_map/all_to_all | solution.py:43
  205.7 3.0 copy-start.11
  258.4 6.6 %copy-start.6 = (bf16[512,2048]{1,0:T(8,128)(2,1)S(1)}, bf16[512,2048]{1,0:T(8,128)(2,1)}, u32[]{:S(2)}) copy-start(bf16[512,2048]{1,0:T(8,128)(2,1)} %reshape_reshape.7) | copy-start | bytes 6291460
  279.1 5.1 %copy-start.10 = (s32[1,128,2]{1,2,0:T(2,128)S(1)}, s32[1,128,2]{1,2,0:T(2,128)}, u32[]{:S(2)}) copy-start(s32[1,128,2]{1,2,0:T(2,128)} %param.32) | copy-start | bytes 3076
  279.1 5.3 %copy-start.12 = (f32[1,128,4]{1,2,0:T(4,128)S(1)}, f32[1,128,4]{1,2,0:T(4,128)}, u32[]{:S(2)}) copy-start(f32[1,128,4]{1,2,0:T(4,128)} %param.30) | copy-start | bytes 6148
  279.1 5.3 %copy-start.13 = (f32[1,128,2]{1,2,0:T(2,128)S(1)}, f32[1,128,2]{1,2,0:T(2,128)}, u32[]{:S(2)}) copy-start(f32[1,128,2]{1,2,0:T(2,128)} %param.31) | copy-start | bytes 3076
  279.1 35.1 %all-to-all-start.5 = ((bf16[128,1,1,4,2048]{4,3,2,1,0:T(4,128)(2,1)}), bf16[128,1,1,4,2048]{4,3,2,1,0:T(4,128)(2,1)S(1)}, u32[]{:S(2)}, u32[]{:S(2)}) async-start(bf16[128,1,1,4,2048]{4,3,2,1,0:T(4,128)(2,1)} %bitcast.277), calls=%async_computation.5 | async-start | bytes 4194304 | tf_op jit(solution)/shard_map/all_to_all | solution.py:58
  314.2 1.3 copy-start.1
where the time goes:
time: 334 us; the launch traced here: 328 us
  other arithmetic  96.3 us (29%)
  local copies, waits for them, and re-layouts  62.7 us (19%)
  waiting for transfers between devices  54.9 us (16%)
  matrix products  44.2 us (13%)
  blocking collectives  40.4 us (12%)
  starting transfers between devices  27.3 us (8%)
    another operation x3, other arithmetic, block_terms(): jax.scipy.linalg.solve_triangular(lower, rhs, lower=True, unit_diagonal=T...  68.5 us
    all_to_all x1, blocking collectives, one_exchange(): parts = lax.all_to_all(parts, axis, split_axis=0, concat_axis=0, tiled=True)  40.4 us
    all_to_all x1, waiting for transfers between devices, one_exchange(): parts = lax.all_to_all(parts, axis, split_axis=0, concat_axis=0, tiled=True)  29.6 us
    all_to_all x2, starting transfers between devices, sent_together(): lax.all_to_all(both, axis, split_axis=split_dim, concat_axis=concat_dim,...  15.5 us
    all_to_all x2, waiting for transfers between devices, sent_together(): lax.all_to_all(both, axis, split_axis=split_dim, concat_axis=concat_dim,...  14.6 us
    unnamed x37, local copies, waits for them, and re-layouts  11.9 us
    all_to_all x2, waiting for transfers between devices, turned_blocks(): result = lax.all_to_all(result, axes[k], k, k, tiled=True)  10.7 us
    dot_general x1, matrix products, expert_apply(): jnp.dot(hidden, down_weight[0], preferred_element_type=jnp.float32)  9.91 us
  transfers between devices with their start and end apart: 5, of which 4 were waited for; matrix products, arithmetic and copies ran while one was open for 4% of the time, Pallas kernels for 0%

commit v1 on v0

v1 whole, which is shorter than its diff:
```python
import jax
import jax.numpy as jnp
from jax import lax
from jax.experimental import pallas as pl
from jax.experimental.pallas import tpu as pltpu
from jax.sharding import PartitionSpec as P

F32 = jnp.float32
BF16 = jnp.bfloat16
MESH = pl.DeviceIdType.MESH
EPS = 1e-06
T = 128
HD = 64
NH = 16
D = 2048
HALF = D // 2
FF = 1024
NE = 128
CHUNKS = 4
PER = NE // CHUNKS


def coords():
    sp = lax.axis_index("sp")
    dp = lax.axis_index("dp")
    return sp >> 2, sp & 3, dp >> 1, dp & 1


def at(z, x, y, c):
    return (((z & 3) << 2) + (x & 3), ((y & 3) << 1) + (c & 1))


def offset(i):
    chunk = i >> 5
    dx = (i >> 3) & 3
    dy = (i >> 1) & 3
    return (chunk - dx - dy) & 3, dx, dy, i & 1


def iota(shape, dim):
    return lax.broadcasted_iota(jnp.int32, shape, dim)


def split(a):
    hi = a.astype(BF16)
    return hi, (a - hi.astype(F32)).astype(BF16)


def dot(a, b):
    return jnp.dot(a, b, preferred_element_type=F32)


def dot3(a, b):
    (ah, al), (bh, bl) = a, b
    return dot(jnp.concatenate([ah, ah, al], axis=1), jnp.concatenate([bh, bl, bh], axis=0))


def roll64(a):
    return pltpu.roll(a, 64, 1)


def kernel(
    small_ref, rate_ref, hgain_ref, egain_ref,
    q_hbm, k_hbm, v_hbm, gate_hbm, res_hbm, om_hbm, wg_hbm, wu_hbm, wd_hbm,
    out_ref,
    q_ref, k_ref, v_ref, gate_ref, res_ref, om_ref, wg_ref, wu_ref, wd_ref,
    rates, raw, kt_ref, rhs_v, rhs_k, qroll, silu_g, cols, rows_ref,
    mb_out, mb_in, s_out, s_in, oloc, pbuf, gated, mixed, x2,
    sel, wsel, out_buf, arrived, prod, back, xs, acc,
    load_sem, rate_sem, mb_sem, s_sem, fwd_send, fwd_recv, ret_send, ret_recv, all_in,
):
    z, x, y, c = coords()
    sp = (z << 2) + x
    partner = at(z, x, y, c + 1)

    loads = [
        pltpu.make_async_copy(src, dst, load_sem.at[i])
        for i, (src, dst) in enumerate(
            (
                (k_hbm, k_ref), (q_hbm, q_ref), (v_hbm, v_ref), (gate_hbm, gate_ref),
                (res_hbm, res_ref), (om_hbm, om_ref),
                (wg_hbm, wg_ref), (wu_hbm, wu_ref), (wd_hbm, wd_ref),
            )
        )
    ]
    for copy in loads:
        copy.start()

    barrier = pltpu.get_barrier_semaphore()

    def greet_sp(i, carry):
        pl.semaphore_signal(barrier, 1, device_id=at(z + (i >> 2), x + i, y, c), device_id_type=MESH)
        return carry

    def greet_dp(i, carry):
        pl.semaphore_signal(barrier, 1, device_id=at(z, x, y + (i >> 1), c + i), device_id_type=MESH)
        return carry

    lax.fori_loop(1, 16, greet_sp, 0)
    lax.fori_loop(1, 8, greet_dp, 0)

    def many_recv(buf, count, sem):
        part = buf.at[pl.ds(0, count)]
        pltpu.make_async_remote_copy(part, part, sem, sem, device_id=partner, device_id_type=MESH).wait_recv()

    def many_sent(buf, count, sem):
        part = buf.at[pl.ds(0, count)]
        pltpu.make_async_remote_copy(part, part, sem, sem, device_id=partner, device_id_type=MESH).wait_send()

    lane = iota((T, T), 1)
    sub = iota((T, T), 0)
    low_half = lane < HD

    small = small_ref[...]
    e0 = small[:, 54:55].astype(jnp.int32)
    e1 = small[:, 55:56].astype(jnp.int32)
    one0 = jnp.where(lane == e0, 1.0, 0.0)
    one1 = jnp.where(lane == e1, 1.0, 0.0)
    before = dot(jnp.where(sub > lane, 1.0, 0.0).astype(BF16), (one0 + one1).astype(BF16))
    rank0 = jnp.sum(before * one0, axis=1, keepdims=True).astype(jnp.int32)
    rank1 = jnp.sum(before * one1, axis=1, keepdims=True).astype(jnp.int32)

    def slot_of(e, rank):
        dz = ((e >> 5) - z) & 3
        dx = ((e >> 3) - x) & 3
        dy = ((e >> 1) - y) & 3
        dc = (e - c) & 1
        return ((((dz + dx + dy) & 3) << 5) + (dx << 3) + (dy << 1) + dc) * 8 + rank

    slot0 = slot_of(e0, rank0)
    slot1 = slot_of(e1, rank1)
    scores = jnp.exp(small)
    is_group = (lane >= 48) & (lane < 52)
    is_pick = (lane >= 52) & (lane < 54)
    own_group = lane == (e0 >> 5) + 48
    group_sum = jnp.sum(jnp.where(is_group, scores, 0.0), axis=1, keepdims=True)
    group_own = jnp.sum(jnp.where(own_group, scores, 0.0), axis=1, keepdims=True)
    pick_sum = jnp.sum(jnp.where(is_pick, scores, 0.0), axis=1, keepdims=True)
    prob = group_own / group_sum
    w0 = prob * scores[:, 52:53] / pick_sum
    w1 = prob * scores[:, 53:54] / pick_sum
    wide = iota((T, NE * 8), 1)
    for h in range(2):
        w = jnp.where(wide == slot0 + 4 * h, w0, 0.0) + jnp.where(wide == slot1 + 4 * h, w1, 0.0)
        hi, lo = split(w)
        wsel[h * T : (h + 1) * T, :] = hi
        wsel[(2 + h) * T : (3 + h) * T, :] = lo
    slot_cols = jnp.where(lane == 0, slot0.astype(F32), slot1.astype(F32))
    slot_rows = jnp.transpose(slot_cols)
    row0 = slot_rows[0:1, :].astype(jnp.int32)
    row1 = slot_rows[1:2, :].astype(jnp.int32)
    tall = iota((NE * 8, T), 0)
    for h in range(2):
        hit = (tall == row0 + 4 * h) | (tall == row1 + 4 * h)
        sel[:, h * T : (h + 1) * T] = jnp.where(hit, 1.0, 0.0).astype(BF16)

    loads[0].wait()
    loads[1].wait()
    loads[2].wait()
    sums = jnp.zeros((2 * T, T), F32)
    sel_row = iota((2 * T, T), 0)
    sel_lane = iota((2 * T, T), 1)
    sel_head = (sel_row & 127) >> 6
    for j in range(NH // 2):
        cut = slice(j * T, (j + 1) * T)
        kb = k_ref[:, cut]
        qb = q_ref[:, cut]
        k32 = kb.astype(F32)
        q32 = qb.astype(F32)
        hi, lo = split(jnp.concatenate([k32 * k32, q32 * q32], axis=0))
        pick = jnp.where(sel_lane == sel_head + 2 * j, 1.0, 0.0).astype(BF16)
        sums = sums + dot(jnp.concatenate([hi, lo], axis=1), pick)
        kt = jnp.transpose(k32)
        kt_ref[j] = kt
        both = jnp.concatenate(
            [jnp.where(sub < HD, kt, 0.0), jnp.where(sub < HD, 0.0, kt)], axis=1
        ).astype(BF16)
        prods = dot(jnp.concatenate([kb, qb], axis=0), both)
        raw[2 * j] = prods[:, :T]
        raw[2 * j + 1] = prods[:, T:]
        v32 = v_ref[:, cut].astype(F32)
        kr = roll64(k32)
        rhs_v[2 * j] = jnp.where(low_half, v32, 0.0).astype(BF16)
        rhs_v[2 * j + 1] = jnp.where(low_half, 0.0, v32).astype(BF16)
        rhs_k[2 * j] = jnp.where(low_half, 0.0, kr).astype(BF16)
        rhs_k[2 * j + 1] = jnp.where(low_half, kr, 0.0).astype(BF16)
        qroll[j] = roll64(q32)
    inv = lax.rsqrt(sums + EPS)
    rk = inv[:T]
    rq = inv[T:] * (HD**-0.5)
    loads[3].wait()
    for j in range(NH // 2):
        cut = slice(j * T, (j + 1) * T)
        v32 = gate_ref[:, cut].astype(F32)
        silu_g[:, cut] = v32 / (1.0 + jnp.exp(-v32))

    pl.semaphore_wait(barrier, 22)

    def send_rate(i, carry):
        pltpu.make_async_remote_copy(
            rate_ref, rates.at[sp], rate_sem.at[0], rate_sem.at[1],
            device_id=at(z + (i >> 2), x + i, y, c), device_id_type=MESH,
        ).start()
        return carry

    lax.fori_loop(1, 16, send_rate, 0)

    def tell_in(i, carry):
        pl.semaphore_signal(all_in, 1, device_id=at(z, x, y + (i >> 1), c + i), device_id_type=MESH)
        return carry

    lax.fori_loop(1, 8, tell_in, 0)
    rates[sp] = rate_ref[...]
    is_head = lane < NH
    beta = jax.nn.sigmoid(jnp.where(is_head, small, 0.0))
    dl = jnp.where(is_head, pltpu.roll(small, T - 16, 1), 0.0)
    el = jnp.where(is_head, pltpu.roll(small, T - 32, 1), 0.0)
    soft = jax.nn.softplus(dl)
    many_recv(rates, 15, rate_sem.at[1])
    eye16 = iota((NH, T), 0) == iota((NH, T), 1)
    rate_row = jnp.sum(jnp.where(eye16, rates[:, 0, :], 0.0), axis=0, keepdims=True)
    g = jnp.where(is_head, el - rate_row * soft, 0.0)
    g1 = g.astype(BF16)
    rest = g - g1.astype(F32)
    g2, g3 = split(rest)
    tri = jnp.where(sub >= lane, 1.0, 0.0).astype(BF16)
    cumul = dot(jnp.concatenate([tri, tri, tri], axis=1), jnp.concatenate([g1, g2, g3], axis=0))
    packed = (
        jnp.where(is_head, cumul, 0.0)
        + pltpu.roll(jnp.where(is_head, rk, 0.0), 16, 1)
        + pltpu.roll(jnp.where(is_head, beta, 0.0), 32, 1)
        + pltpu.roll(jnp.where(is_head, rq, 0.0), 48, 1)
    )
    rows_ref[...] = jnp.transpose(packed)
    colpack = (
        jnp.where(is_head, cumul, 0.0)
        + pltpu.roll(jnp.where(is_head, beta * rk, 0.0), 16, 1)
        + pltpu.roll(jnp.where(is_head, rq, 0.0), 32, 1)
    )
    cols[0] = colpack
    for n in range(1, 4):
        cols[n] = pltpu.roll(colpack, T - 4 * n, 1)

    def heads(n, carry):
        col = cols.at[n]
        causal = sub >= lane
        ls, atts, ups, ws, kds, tots = [], [], [], [], [], []
        for hh in range(4):
            h = n * 4 + hh
            c_row = rows_ref[pl.ds(h, 1), :]
            k_row = rows_ref[pl.ds(h + 16, 1), :]
            b_row = rows_ref[pl.ds(h + 32, 1), :]
            c_col = col[:, hh : hh + 1]
            dec = jnp.where(causal, jnp.exp(jnp.minimum(c_col - c_row, 0.0)), 0.0) * k_row
            ls.append(jnp.where(sub > lane, raw[h, 0:T, :] * dec * col[:, hh + 16 : hh + 17], 0.0))
            atts.append(raw[h, T : 2 * T, :] * dec * col[:, hh + 32 : hh + 33])
            ups.append(b_row)
            ws.append(b_row * k_row * jnp.exp(c_row))
            last = c_row[:, T - 1 : T]
            kds.append(k_row * jnp.exp(last - c_row))
            tots.append(jnp.exp(last))
        pairs = sub >> 1 == lane >> 1
        ts = [jnp.where(sub == lane, 1.0, 0.0) - jnp.where(pairs, l, 0.0) for l in ls]
        for bits in range(1, 7):
            m = ((sub >> bits) == (lane >> bits) + 1) & (((sub >> bits) & 1) == 1)
            tsp = [split(t) for t in ts]
            xsp = [split(dot3(split(jnp.where(m, l, 0.0)), t)) for l, t in zip(ls, tsp)]
            ts = [t - dot3(tp, xx) for t, tp, xx in zip(ts, tsp, xsp)]
        auws = []
        for hh in range(4):
            h = n * 4 + hh
            uh, ul = split(ts[hh] * ups[hh])
            wh, wl = split(ts[hh] * ws[hh])
            vm = rhs_v[h]
            km = rhs_k[h]
            uw = dot(jnp.concatenate([uh, ul, wh, wl], axis=1), jnp.concatenate([vm, vm, km, km], axis=0))
            ktp = kt_ref[n * 2 + hh // 2, (hh % 2) * HD : (hh % 2) * HD + HD, :]
            both = jnp.concatenate([atts[hh], ktp * kds[hh]], axis=0)
            res = dot3(split(both), split(uw))
            auws.append(res[:T])
            bn = res[T:]
            if hh % 2:
                bn = roll64(bn)
            lane64 = iota((HD, T), 1)
            ident = jnp.where(lane64 - HD == iota((HD, T), 0), tots[hh], 0.0)
            mb_out[h] = jnp.where(lane64 < HD, bn, ident - bn)
        for jj in range(2):
            j = n * 2 + jj
            a, b = 2 * jj, 2 * jj + 1
            sc_a = col[:, a + 32 : a + 33] * jnp.exp(col[:, a : a + 1])
            sc_b = col[:, b + 32 : b + 33] * jnp.exp(col[:, b : b + 1])
            p = qroll[j] * jnp.where(low_half, sc_b, sc_a) - jnp.where(low_half, auws[b], auws[a])
            hi, lo = split(p)
            pbuf[j, :, 0:T] = hi
            pbuf[j, :, T : 2 * T] = lo
            oloc[j] = jnp.where(low_half, auws[a], auws[b])
        for hh in range(4):
            h = n * 4 + hh

            @pl.when(h == sp)
            def _():
                mb_in[h] = mb_out[h]

            @pl.when(h != sp)
            def _():
                pltpu.make_async_remote_copy(
                    mb_out.at[h], mb_in.at[sp], mb_sem.at[0], mb_sem.at[1],
                    device_id=at(n, hh, y, c), device_id_type=MESH,
                ).start()

        return carry

    lax.fori_loop(0, 4, heads, 0)

    many_recv(mb_in, 15, mb_sem.at[1])
    lane64 = iota((HD, T), 1)
    sub64 = iota((HD, T), 0)
    ident = jnp.where((lane64 & 63) == sub64, 1.0, 0.0).astype(BF16)
    mine = (lane64 >> 6) == (sp & 1)
    zero = jnp.zeros((HD, T), BF16)
    place = sp + 1 - 2 * (sp & 1)
    state = jnp.zeros((HD, T), F32)
    for p in range(16):
        s_out[p] = jnp.where(mine, state, 0.0).astype(BF16)

        @pl.when(sp == p)
        def _():
            s_in[place] = s_out[p]

        @pl.when(sp != p)
        def _():
            pltpu.make_async_remote_copy(
                s_out.at[p], s_in.at[place], s_sem.at[0], s_sem.at[1],
                device_id=at(p >> 2, p, y, c), device_id_type=MESH,
            ).start()

        if p < 15:
            sh, sl = split(state)
            state = dot3(
                split(mb_in[p]),
                (jnp.concatenate([ident, sh], axis=0), jnp.concatenate([zero, sl], axis=0)),
            )

    many_recv(s_in, 15, s_sem.at[1])
    ones = jnp.where((iota((2 * T, T), 0) >> 6) & 1 == iota((2 * T, T), 1) >> 6, 1.0, 0.0).astype(BF16)
    for j in range(NH // 2):
        cut = slice(j * T, (j + 1) * T)
        sj = s_in[2 * j : 2 * j + 2].reshape(T, T)
        o = oloc[j] + dot(pbuf[j], jnp.concatenate([sj, sj], axis=0))
        hi, lo = split(o * o)
        mean = dot(jnp.concatenate([hi, lo], axis=1), ones) * (1.0 / HD)
        normed = (o * lax.rsqrt(mean + EPS) * hgain_ref[...]).astype(BF16)
        gated[:, cut] = (normed.astype(F32) * silu_g[:, cut]).astype(BF16)
    loads[4].wait()
    loads[5].wait()
    total = jnp.zeros((T, 1), F32)
    for n in range(4):
        cut = slice(n * 512, (n + 1) * 512)
        m = res_ref[:, cut].astype(F32) + dot(gated[...], om_ref[:, cut])
        mixed[:, cut] = m
        total = total + jnp.sum(m * m, axis=1, keepdims=True)
    inv = lax.rsqrt(total * (1.0 / D) + EPS)
    for h in range(2):
        cut = slice(h * HALF, (h + 1) * HALF)
        x2[h * T : (h + 1) * T, :] = (mixed[:, cut] * inv * egain_ref[:, cut]).astype(BF16)

    pl.semaphore_wait(all_in, 7)

    def dispatch(n, carry):
        block = dot(sel[pl.ds(n * 256, 256), :], x2[...]).astype(BF16)
        out_buf[pl.ds(n * PER, PER)] = block.reshape(PER, 8, HALF)

        def send(j, inner):
            i = n * PER + j
            dz, dx, dy, dc = offset(i)

            @pl.when(i != 0)
            def _():
                pltpu.make_async_remote_copy(
                    out_buf.at[i], arrived.at[i], fwd_send, fwd_recv.at[n],
                    device_id=at(z + dz, x + dx, y + dy, c + dc), device_id_type=MESH,
                ).start()

            return inner

        lax.fori_loop(0, PER, send, 0)
        return carry

    lax.fori_loop(0, CHUNKS, dispatch, 0)
    arrived[0] = out_buf[0]
    loads[6].wait()
    loads[7].wait()
    loads[8].wait()

    sub256 = iota((256, 256), 0)
    lane256 = iota((256, 256), 1)
    source = ((sub256 & 127) >> 2) * 8 + (sub256 >> 7) * 4 + (sub256 & 3)
    apart = jnp.where(source == lane256, 1.0, 0.0).astype(BF16)
    source = ((lane256 & 127) >> 2) * 8 + (lane256 >> 7) * 4 + (lane256 & 3)
    together = jnp.where(source == sub256, 1.0, 0.0).astype(BF16)

    def expert(n, carry):
        @pl.when(n == 0)
        def _():
            many_recv(arrived, PER - 1, fwd_recv.at[0])

        @pl.when(n != 0)
        def _():
            many_recv(arrived, PER, fwd_recv.at[n])

        rows = arrived[pl.ds(n * PER, PER)].reshape(256, HALF)
        xs[...] = dot(apart, rows).astype(BF16)
        for k in range(4):
            cut = slice(k * 256, (k + 1) * 256)
            gate = dot(xs[0:T, :], wg_ref[0:HALF, cut]) + dot(xs[T : 2 * T, :], wg_ref[HALF:D, cut])
            upper = dot(xs[0:T, :], wu_ref[0:HALF, cut]) + dot(xs[T : 2 * T, :], wu_ref[HALF:D, cut])
            acc[:, cut] = (gate / (1.0 + jnp.exp(-gate)) * upper).astype(BF16)
        for k in range(8):
            cut = slice(k * 256, (k + 1) * 256)
            half, inside = k // 4, slice((k % 4) * 256, (k % 4 + 1) * 256)
            xs[half * T : (half + 1) * T, inside] = dot(acc[...], wd_ref[:, cut]).astype(BF16)
        prod[pl.ds(n * PER, PER)] = dot(together, xs[...]).astype(BF16).reshape(PER, 8, HALF)

        def send(j, inner):
            i = n * PER + j
            dz, dx, dy, dc = offset(i)

            @pl.when(i != 0)
            def _():
                pltpu.make_async_remote_copy(
                    prod.at[i], back.at[i], ret_send, ret_recv.at[n],
                    device_id=at(z - dz, x - dx, y - dy, c - dc), device_id_type=MESH,
                ).start()

            return inner

        lax.fori_loop(0, PER, send, 0)
        return carry

    lax.fori_loop(0, CHUNKS, expert, 0)
    back[0] = prod[0]

    for n in range(CHUNKS):
        many_recv(back, PER - 1 if n == 0 else PER, ret_recv.at[n])
        part = dot(wsel[:, n * 256 : (n + 1) * 256], back[n * PER : (n + 1) * PER].reshape(256, HALF))
        for h in range(2):
            cut = slice(h * HALF, (h + 1) * HALF)
            total = mixed[:, cut] + (part[h * T : (h + 1) * T] + part[(2 + h) * T : (3 + h) * T])
            if n < CHUNKS - 1:
                mixed[:, cut] = total
            else:
                out_ref[:, cut] = total.astype(BF16)

    many_sent(rates, 15, rate_sem.at[0])
    many_sent(mb_out, 15, mb_sem.at[0])
    many_sent(s_out, 15, s_sem.at[0])
    many_sent(out_buf, NE - 1, fwd_send)
    many_sent(prod, NE - 1, ret_send)


def call(small, rate, hgain, egain, *big):
    vm = pl.BlockSpec(memory_space=pltpu.VMEM)
    hbm = pl.BlockSpec(memory_space=pl.ANY)
    return pl.pallas_call(
        kernel,
        out_shape=jax.ShapeDtypeStruct((T, D), BF16),
        in_specs=[vm] * 4 + [hbm] * 9,
        out_specs=vm,
        scratch_shapes=[
            pltpu.VMEM((T, NH * HD), BF16),
            pltpu.VMEM((T, NH * HD), BF16),
            pltpu.VMEM((T, NH * HD), BF16),
            pltpu.VMEM((T, NH * HD), BF16),
            pltpu.VMEM((T, D), BF16),
            pltpu.VMEM((NH * HD, D), BF16),
            pltpu.VMEM((D, FF), BF16),
            pltpu.VMEM((D, FF), BF16),
            pltpu.VMEM((FF, D), BF16),
            pltpu.VMEM((16, 8, T), F32),
            pltpu.VMEM((NH, 2 * T, T), F32),
            pltpu.VMEM((NH // 2, T, T), F32),
            pltpu.VMEM((NH, T, T), BF16),
            pltpu.VMEM((NH, T, T), BF16),
            pltpu.VMEM((NH // 2, T, T), F32),
            pltpu.VMEM((T, NH * HD), F32),
            pltpu.VMEM((4, T, T), F32),
            pltpu.VMEM((T, T), F32),
            pltpu.VMEM((NH, HD, T), F32),
            pltpu.VMEM((NH, HD, T), F32),
            pltpu.VMEM((NH, HD, T), BF16),
            pltpu.VMEM((NH, HD, T), BF16),
            pltpu.VMEM((NH // 2, T, T), F32),
            pltpu.VMEM((NH // 2, T, 2 * T), BF16),
            pltpu.VMEM((T, NH * HD), BF16),
            pltpu.VMEM((T, D), F32),
            pltpu.VMEM((2 * T, HALF), BF16),
            pltpu.VMEM((NE * 8, 2 * T), BF16),
            pltpu.VMEM((4 * T, NE * 8), BF16),
            pltpu.VMEM((NE, 8, HALF), BF16),
            pltpu.VMEM((NE, 8, HALF), BF16),
            pltpu.VMEM((NE, 8, HALF), BF16),
            pltpu.VMEM((NE, 8, HALF), BF16),
            pltpu.VMEM((2 * T, HALF), BF16),
            pltpu.VMEM((T, FF), BF16),
            pltpu.SemaphoreType.DMA((9,)),
            pltpu.SemaphoreType.DMA((2,)),
            pltpu.SemaphoreType.DMA((2,)),
            pltpu.SemaphoreType.DMA((2,)),
            pltpu.SemaphoreType.DMA,
            pltpu.SemaphoreType.DMA((CHUNKS,)),
            pltpu.SemaphoreType.DMA,
            pltpu.SemaphoreType.DMA((CHUNKS,)),
            pltpu.SemaphoreType.REGULAR,
        ],
        compiler_params=pltpu.CompilerParams(
            collective_id=0, has_side_effects=True, vmem_limit_bytes=60 * 1024 * 1024
        ),
        name="layer",
    )(small, rate, hgain, egain, *big)


def shards(
    residual, query, key, value, output_gate, write_logits, decay_logits, extra_decay, head_rate,
    head_gain, output_matrix, expert_gain, group_scores, expert_scores, routes,
    gate_weight, up_weight, down_weight,
):
    small = jnp.concatenate(
        [
            write_logits[0], decay_logits[0], extra_decay[0], group_scores[0], expert_scores[0],
            routes[0].astype(F32), jnp.zeros((T, T - 56), F32),
        ],
        axis=1,
    )
    rate = jnp.broadcast_to(head_rate[:, None], (8, T))
    hgain = jnp.tile(head_gain, 2)[None]
    out = call(
        small, rate, hgain, expert_gain[None], query[0], key[0], value[0], output_gate[0],
        residual[0], output_matrix, gate_weight[0], up_weight[0], down_weight[0],
    )
    return out[None]


def solution(mesh):
    tok = P("dp", "sp", None)
    exp = P(("sp", "dp"), None, None)
    in_specs = (
        (tok,) * 8 + (P("sp"), P(), P(), P()) + (tok,) * 3 + (exp,) * 3
    )
    return jax.shard_map(shards, mesh=mesh, in_specs=in_specs, out_specs=tok, check_vma=False)
```

time: 334 us -> 106 us (0.32); the launches traced: 328 us -> 106 us
  other arithmetic: 96.3 us -> 0.01 us
  Pallas kernels: 0 us -> 95.8 us
  waiting for transfers between devices: 54.9 us -> 0 us
  local copies, waits for them, and re-layouts: 62.7 us -> 9.27 us
  matrix products: 44.2 us -> 0 us
  blocking collectives: 40.4 us -> 0 us
  starting transfers between devices: 27.3 us -> 0 us
    pallas_call x0 -> x1, Pallas kernels: none -> 95.8 us  [call(): pl.pallas_call(kernel, out_shape=jax.ShapeDtypeStruct((T, D), BF16), in_s...]
    another operation x7 -> x0, other arithmetic: 69 us -> none  [the longest x3 68.5 us: block_terms(): jax.scipy.linalg.solve_triangular(lower, rhs, lower=True, unit_diagonal=T...]
    all_to_all x5 -> x0, waiting for transfers between devices: 54.9 us -> none  [the longest x1 29.6 us: one_exchange(): parts = lax.all_to_all(parts, axis, split_axis=0, concat_axis=0, tiled=True)]
    dot_general x23 -> x0, matrix products: 42.9 us -> none  [the longest x1 9.91 us: expert_apply(): jnp.dot(hidden, down_weight[0], preferred_element_type=jnp.float32)]
    all_to_all x1 -> x0, blocking collectives: 40.4 us -> none  [one_exchange(): parts = lax.all_to_all(parts, axis, split_axis=0, concat_axis=0, tiled=True)]
    all_to_all x5 -> x0, starting transfers between devices: 27.3 us -> none  [the longest x2 15.5 us: sent_together(): lax.all_to_all(both, axis, split_axis=split_dim, concat_axis=concat_dim,...]
    mul x6 -> x0, other arithmetic: 11.9 us -> none  [the longest x1 7.46 us: block_terms(): jnp.einsum('nid,njd->nij', qb, kb, precision=highest_precision) * decay]
    another operation x9 -> x2, local copies, waits for them, and re-layouts: 11.9 us -> 1.24 us  [shards(): hgain = jnp.tile(head_gain, 2)[None]]
  transfers between devices with their start and end apart: 5 -> 0, of which waited for: 4 -> 0; matrix products, arithmetic and copies ran while one was open for 4% -> 0% of each run, Pallas kernels for 0% -> 0%
where the time goes in v1:
time: 106 us
  Pallas kernels  95.8 us (90%)
  local copies, waits for them, and re-layouts  9.27 us (9%)
    pallas_call x1, Pallas kernels, call(): pl.pallas_call(kernel, out_shape=jax.ShapeDtypeStruct((T, D), BF16), in_s...  95.8 us
    unnamed x7, local copies, waits for them, and re-layouts  6.63 us

profile of v1, /device:TPU:1, one launch (start us, length us, event | category | flops | bytes accessed | tf_op | source)
XLA Modules:
  0.0 105.8 jit_solution(15551478923423563984)
XLA Ops:
  0.7 0.7 tile.2
  1.3 0.6 broadcast_in_dim_tile.3.hgain_ref
  1.9 0.6 broadcast_in_dim.19.rate_ref
  2.5 0.8 copy.19
  3.3 0.8 copy.20
  4.1 0.8 copy.21
  4.9 0.8 copy.22
  5.7 0.8 copy.23
  6.5 0.8 copy.24
  7.3 0.8 concatenate.3.small_ref
  8.1 95.8 %layer.1 = bf16[128,2048]{1,0:T(8,128)(2,1)} custom-call(f32[128,128]{1,0:T(8,128)} %concatenate.3.small_ref, f32[8,128]{1,0:T(8,128)} %broadcast_in_dim.19.rate_ref, f32[1,128]{1,0:T(1,128)} %broadcast_in_dim_tile.3.hgain_ref, f32[1,2048]{1,0:T(1,128)} %bitcast.33, bf16[128,1024]{1,0:T(8,128)(2,1)} %bitcast.24, bf16[128,1024]{1,0:T(8,128)(2,1)} %bitcast.25, ...), custom_call_target="tpu_custom_call" | custom-call | tf_op jit(solution)/shard_map/layer/pallas_call | solution.py:464
  103.9 1.9 %copy.27 = bf16[1,128,2048]{2,1,0:T(8,128)(2,1)} copy(bf16[1,128,2048]{2,1,0:T(8,128)(2,1)} %bitcast.22) | data formatting | bytes 1048576
  (2 shorter events, 0.0 us)

commit v2 on v1

--- a/solution.py
+++ b/solution.py
@@ -55,17 +55,37 @@
     return dot(jnp.concatenate([ah, ah, al], axis=1), jnp.concatenate([bh, bl, bh], axis=0))
 
 
+def dot4(a, b):
+    (ah, al), (bh, bl) = a, b
+    left = jnp.concatenate(
+        [jnp.concatenate([ah, ah], axis=1), jnp.concatenate([al, al], axis=1)], axis=0
+    )
+    both = dot(left, jnp.concatenate([bh, bl], axis=0))
+    return both[: ah.shape[0]] + both[ah.shape[0] :]
+
+
+def odd_blocks(a, size):
+    return jnp.concatenate([a[i : i + size] for i in range(size, T, 2 * size)], axis=0)
+
+
+def with_odd_blocks(even, odd, size):
+    parts = []
+    for n, i in enumerate(range(0, T, 2 * size)):
+        parts += [even[i : i + size], odd[n * size : (n + 1) * size]]
+    return jnp.concatenate(parts, axis=0)
+
+
 def roll64(a):
     return pltpu.roll(a, 64, 1)
 
 
 def kernel(
-    small_ref, rate_ref, hgain_ref, egain_ref,
+    wsl_ref, dl_ref, el_ref, grs_ref, ces_ref, routes_ref, rate_in, hg_ref, egain_ref,
     q_hbm, k_hbm, v_hbm, gate_hbm, res_hbm, om_hbm, wg_hbm, wu_hbm, wd_hbm,
     out_ref,
     q_ref, k_ref, v_ref, gate_ref, res_ref, om_ref, wg_ref, wu_ref, wd_ref,
-    rates, raw, kt_ref, rhs_v, rhs_k, qroll, silu_g, cols, rows_ref,
-    mb_out, mb_in, s_out, s_in, oloc, pbuf, gated, mixed, x2,
+    small_rows, rate_ref, hgain_ref, rates, raw, kt_ref, rhs_v, rhs_k, qroll, silu_g, cols, rows_ref,
+    uwbuf, mb_out, mb_in, s_out, s_in, oloc, pbuf, gated, mixed, x2,
     sel, wsel, out_buf, arrived, prod, back, xs, acc,
     load_sem, rate_sem, mb_sem, s_sem, fwd_send, fwd_recv, ret_send, ret_recv, all_in,
 ):
@@ -111,7 +131,17 @@
     sub = iota((T, T), 0)
     low_half = lane < HD
 
-    small = small_ref[...]
+    rate_ref[...] = jnp.full((8, T), rate_in[0], F32)
+    hgain_ref[:, 0:HD] = hg_ref[...]
+    hgain_ref[:, HD:T] = hg_ref[...]
+    small_rows[...] = jnp.zeros((T, T), F32)
+    small_rows[0:16, :] = wsl_ref[...]
+    small_rows[16:32, :] = dl_ref[...]
+    small_rows[32:48, :] = el_ref[...]
+    small_rows[48:52, :] = grs_ref[...]
+    small_rows[52:54, :] = ces_ref[...]
+    small_rows[54:56, :] = routes_ref[...].astype(F32)
+    small = jnp.transpose(small_rows[...])
     e0 = small[:, 54:55].astype(jnp.int32)
     e1 = small[:, 55:56].astype(jnp.int32)
     one0 = jnp.where(lane == e0, 1.0, 0.0)
@@ -241,10 +271,14 @@
     for n in range(1, 4):
         cols[n] = pltpu.roll(colpack, T - 4 * n, 1)
 
-    def heads(n, carry):
+    lane64 = iota((HD, T), 1)
+    sub64 = iota((HD, T), 0)
+
+    def heads(step, carry):
+        n = (z + 3 - step) & 3
         col = cols.at[n]
         causal = sub >= lane
-        ls, atts, ups, ws, kds, tots = [], [], [], [], [], []
+        ls, ups, ws, kds, tots = [], [], [], [], []
         for hh in range(4):
             h = n * 4 + hh
             c_row = rows_ref[pl.ds(h, 1), :]
@@ -253,20 +287,34 @@
             c_col = col[:, hh : hh + 1]
             dec = jnp.where(causal, jnp.exp(jnp.minimum(c_col - c_row, 0.0)), 0.0) * k_row
             ls.append(jnp.where(sub > lane, raw[h, 0:T, :] * dec * col[:, hh + 16 : hh + 17], 0.0))
-            atts.append(raw[h, T : 2 * T, :] * dec * col[:, hh + 32 : hh + 33])
+            raw[h, T : 2 * T, :] = raw[h, T : 2 * T, :] * dec * col[:, hh + 32 : hh + 33]
             ups.append(b_row)
             ws.append(b_row * k_row * jnp.exp(c_row))
             last = c_row[:, T - 1 : T]
             kds.append(k_row * jnp.exp(last - c_row))
             tots.append(jnp.exp(last))
-        pairs = sub >> 1 == lane >> 1
-        ts = [jnp.where(sub == lane, 1.0, 0.0) - jnp.where(pairs, l, 0.0) for l in ls]
-        for bits in range(1, 7):
-            m = ((sub >> bits) == (lane >> bits) + 1) & (((sub >> bits) & 1) == 1)
-            tsp = [split(t) for t in ts]
-            xsp = [split(dot3(split(jnp.where(m, l, 0.0)), t)) for l, t in zip(ls, tsp)]
-            ts = [t - dot3(tp, xx) for t, tp, xx in zip(ts, tsp, xsp)]
-        auws = []
+        ts = []
+        pairs = (sub >> 1) == (lane >> 1)
+        m = ((sub >> 1) == (lane >> 1) + 1) & (((sub >> 1) & 1) == 1)
+        for l in ls:
+            near = jnp.where(pairs, l, 0.0)
+            far = jnp.where(m, l, 0.0)
+            far = far - pltpu.roll(far, T - 1, 1) * jnp.sum(near, axis=0, keepdims=True)
+            far = far - pltpu.roll(far, 1, 0) * jnp.sum(near, axis=1, keepdims=True)
+            ts.append(jnp.where(sub == lane, 1.0, 0.0) - near - far)
+        m = ((sub >> 2) == (lane >> 2) + 1) & (((sub >> 2) & 1) == 1)
+        tsp = [split(t) for t in ts]
+        xsp = [split(dot3(split(jnp.where(m, l, 0.0)), t)) for l, t in zip(ls, tsp)]
+        ts = [t - dot3(tp, xx) for t, tp, xx in zip(ts, tsp, xsp)]
+        for bits in range(3, 7):
+            size = 1 << bits
+            m = (lane64 >> bits) == 2 * (sub64 >> bits)
+            none = jnp.zeros((T, T), F32)
+            xs_ = [dot4(split(jnp.where(m, odd_blocks(l, size), 0.0)), split(t)) for l, t in zip(ls, ts)]
+            odd = [odd_blocks(t, size) for t in ts]
+            ys_ = [dot4(split(o), split(with_odd_blocks(none, x_, size))) for o, x_ in zip(odd, xs_)]
+            ts = [with_odd_blocks(t, o - y_, size) for t, o, y_ in zip(ts, odd, ys_)]
+        uws = []
         for hh in range(4):
             h = n * 4 + hh
             uh, ul = split(ts[hh] * ups[hh])
@@ -274,16 +322,42 @@
             vm = rhs_v[h]
             km = rhs_k[h]
             uw = dot(jnp.concatenate([uh, ul, wh, wl], axis=1), jnp.concatenate([vm, vm, km, km], axis=0))
+            uws.append(split(uw))
+            uwbuf[h, 0:T, :] = uws[hh][0]
+            uwbuf[h, T : 2 * T, :] = uws[hh][1]
+        for hh in range(4):
+            h = n * 4 + hh
             ktp = kt_ref[n * 2 + hh // 2, (hh % 2) * HD : (hh % 2) * HD + HD, :]
-            both = jnp.concatenate([atts[hh], ktp * kds[hh]], axis=0)
-            res = dot3(split(both), split(uw))
-            auws.append(res[:T])
-            bn = res[T:]
+            bn = dot4(split(ktp * kds[hh]), uws[hh])
             if hh % 2:
                 bn = roll64(bn)
-            lane64 = iota((HD, T), 1)
-            ident = jnp.where(lane64 - HD == iota((HD, T), 0), tots[hh], 0.0)
+            ident = jnp.where(lane64 - HD == sub64, tots[hh], 0.0)
             mb_out[h] = jnp.where(lane64 < HD, bn, ident - bn)
+        for hh in range(4):
+            h = n * 4 + hh
+
+            @pl.when(h == sp)
+            def _():
+                mb_in[h] = mb_out[h]
+
+            @pl.when(h != sp)
+            def _():
+                pltpu.make_async_remote_copy(
+                    mb_out.at[h], mb_in.at[sp], mb_sem.at[0], mb_sem.at[1],
+                    device_id=at(n, hh, y, c), device_id_type=MESH,
+                ).start()
+
+        return carry
+
+    lax.fori_loop(0, 4, heads, 0)
+
+    def inside(n, carry):
+        col = cols.at[n]
+        auws = []
+        for hh in range(4):
+            h = n * 4 + hh
+            uw = uwbuf[h]
+            auws.append(dot3(split(raw[h, T : 2 * T, :]), (uw[:T], uw[T:])))
         for jj in range(2):
             j = n * 2 + jj
             a, b = 2 * jj, 2 * jj + 1
@@ -294,58 +368,83 @@
             pbuf[j, :, 0:T] = hi
             pbuf[j, :, T : 2 * T] = lo
             oloc[j] = jnp.where(low_half, auws[a], auws[b])
-        for hh in range(4):
-            h = n * 4 + hh
-
-            @pl.when(h == sp)
-            def _():
-                mb_in[h] = mb_out[h]
-
-            @pl.when(h != sp)
-            def _():
-                pltpu.make_async_remote_copy(
-                    mb_out.at[h], mb_in.at[sp], mb_sem.at[0], mb_sem.at[1],
-                    device_id=at(n, hh, y, c), device_id_type=MESH,
-                ).start()
-
-        return carry
-
-    lax.fori_loop(0, 4, heads, 0)
+        return carry
+
+    lax.fori_loop(0, 4, inside, 0)
 
     many_recv(mb_in, 15, mb_sem.at[1])
-    lane64 = iota((HD, T), 1)
-    sub64 = iota((HD, T), 0)
-    ident = jnp.where((lane64 & 63) == sub64, 1.0, 0.0).astype(BF16)
-    mine = (lane64 >> 6) == (sp & 1)
+    first = lane64 < HD
+    eye = (lane64 & 63) == sub64
+    ident_two = jnp.where(eye, 1.0, 0.0).astype(BF16)
+    ident_one = jnp.where(eye & first, 1.0, 0.0).astype(BF16)
     zero = jnp.zeros((HD, T), BF16)
-    place = sp + 1 - 2 * (sp & 1)
-    state = jnp.zeros((HD, T), F32)
-    for p in range(16):
-        s_out[p] = jnp.where(mine, state, 0.0).astype(BF16)
-
-        @pl.when(sp == p)
-        def _():
-            s_in[place] = s_out[p]
-
-        @pl.when(sp != p)
-        def _():
-            pltpu.make_async_remote_copy(
-                s_out.at[p], s_in.at[place], s_sem.at[0], s_sem.at[1],
-                device_id=at(p >> 2, p, y, c), device_id_type=MESH,
-            ).start()
-
-        if p < 15:
-            sh, sl = split(state)
-            state = dot3(
-                split(mb_in[p]),
-                (jnp.concatenate([ident, sh], axis=0), jnp.concatenate([zero, sl], axis=0)),
-            )
+
+    def after(later, earlier, ident):
+        hi, lo = split(earlier)
+        return dot4(
+            later, (jnp.concatenate([ident, hi], axis=0), jnp.concatenate([zero, lo], axis=0))
+        )
+
+    def added(step):
+        return jnp.where(first, step, roll64(step))
+
+    def keep(p, state):
+        s_out[p] = jnp.where(first[: HD // 2], state[: HD // 2], state[HD // 2 :]).astype(BF16)
+
+    steps = [mb_in[p] for p in range(15)]
+    ones_ = [split(m) for m in steps]
+    twos = [after(ones_[2 * i + 1], steps[2 * i], ident_one) for i in range(7)]
+    twos_ = [split(m) for m in twos]
+    fours = [after(twos_[2 * i + 1], twos[2 * i], ident_one) for i in range(3)]
+    keep(0, jnp.zeros((HD, T), F32))
+    state = added(fours[0])
+    keep(1, added(steps[0]))
+    two = added(twos[0])
+    keep(2, two)
+    keep(3, after(ones_[2], two, ident_two))
+    keep(4, state)
+    eight = after(split(fours[1]), state, ident_two)
+    six = after(twos_[2], state, ident_two)
+    keep(5, after(ones_[4], state, ident_two))
+    keep(6, six)
+    keep(7, after(ones_[6], six, ident_two))
+    keep(8, eight)
+    twelve = after(split(fours[2]), eight, ident_two)
+    ten = after(twos_[4], eight, ident_two)
+    keep(9, after(ones_[8], eight, ident_two))
+    keep(10, ten)
+    fourteen = after(twos_[6], twelve, ident_two)
+    keep(11, after(ones_[10], ten, ident_two))
+    keep(12, twelve)
+    keep(13, after(ones_[12], twelve, ident_two))
+    keep(14, fourteen)
+    keep(15, after(ones_[14], fourteen, ident_two))
+
+    def send_state(i, carry):
+        p = (sp + i) & 15
+        pltpu.make_async_remote_copy(
+            s_out.at[p], s_in.at[sp], s_sem.at[0], s_sem.at[1],
+            device_id=at(p >> 2, p, y, c), device_id_type=MESH,
+        ).start()
+        return carry
+
+    lax.fori_loop(1, 16, send_state, 0)
+    s_in[sp] = s_out[sp]
 
     many_recv(s_in, 15, s_sem.at[1])
     ones = jnp.where((iota((2 * T, T), 0) >> 6) & 1 == iota((2 * T, T), 1) >> 6, 1.0, 0.0).astype(BF16)
     for j in range(NH // 2):
         cut = slice(j * T, (j + 1) * T)
-        sj = s_in[2 * j : 2 * j + 2].reshape(T, T)
+        even = s_in[2 * j].astype(F32)
+        odd = s_in[2 * j + 1].astype(F32)
+        head = first[: HD // 2]
+        sj = jnp.concatenate(
+            [
+                jnp.where(head, 0.0, roll64(odd)), jnp.where(head, 0.0, odd),
+                jnp.where(head, even, 0.0), jnp.where(head, roll64(even), 0.0),
+            ],
+            axis=0,
+        ).astype(BF16)
         o = oloc[j] + dot(pbuf[j], jnp.concatenate([sj, sj], axis=0))
         hi, lo = split(o * o)
         mean = dot(jnp.concatenate([hi, lo], axis=1), ones) * (1.0 / HD)
@@ -399,6 +498,21 @@
     source = ((lane256 & 127) >> 2) * 8 + (lane256 >> 7) * 4 + (lane256 & 3)
     together = jnp.where(source == sub256, 1.0, 0.0).astype(BF16)
 
+    def send_back(n):
+        def send(j, inner):
+            i = n * PER + j
+            dz, dx, dy, dc = offset(i)
+
+            @pl.when(i != 0)
+            def _():
+                pltpu.make_async_remote_copy(
+                    prod.at[i], back.at[i], ret_send, ret_recv.at[n],
+                    device_id=at(z - dz, x - dx, y - dy, c - dc), device_id_type=MESH,
+                ).start()
+
+            return inner
+
+        lax.fori_loop(0, PER, send, 0)
     def expert(n, carry):
         @pl.when(n == 0)
         def _():
@@ -421,23 +535,14 @@
             xs[half * T : (half + 1) * T, inside] = dot(acc[...], wd_ref[:, cut]).astype(BF16)
         prod[pl.ds(n * PER, PER)] = dot(together, xs[...]).astype(BF16).reshape(PER, 8, HALF)
 
-        def send(j, inner):
-            i = n * PER + j
-            dz, dx, dy, dc = offset(i)
-
-            @pl.when(i != 0)
-            def _():
-                pltpu.make_async_remote_copy(
-                    prod.at[i], back.at[i], ret_send, ret_recv.at[n],
-                    device_id=at(z - dz, x - dx, y - dy, c - dc), device_id_type=MESH,
-                ).start()
-
-            return inner
-
-        lax.fori_loop(0, PER, send, 0)
+        @pl.when(n >= 1)
+        def _():
+            send_back(n - 1)
+
         return carry
 
     lax.fori_loop(0, CHUNKS, expert, 0)
+    send_back(3)
     back[0] = prod[0]
 
     for n in range(CHUNKS):
@@ -458,13 +563,13 @@
     many_sent(prod, NE - 1, ret_send)
 
 
-def call(small, rate, hgain, egain, *big):
+def call(*args):
     vm = pl.BlockSpec(memory_space=pltpu.VMEM)
     hbm = pl.BlockSpec(memory_space=pl.ANY)
     return pl.pallas_call(
         kernel,
-        out_shape=jax.ShapeDtypeStruct((T, D), BF16),
-        in_specs=[vm] * 4 + [hbm] * 9,
+        out_shape=pltpu.VMEM((T, D), BF16),
+        in_specs=[vm] * 6 + [pl.BlockSpec(memory_space=pltpu.SMEM)] + [vm] * 2 + [hbm] * 9,
         out_specs=vm,
         scratch_shapes=[
             pltpu.VMEM((T, NH * HD), BF16),
@@ -476,6 +581,9 @@
             pltpu.VMEM((D, FF), BF16),
             pltpu.VMEM((D, FF), BF16),
             pltpu.VMEM((FF, D), BF16),
+            pltpu.VMEM((T, T), F32),
+            pltpu.VMEM((8, T), F32),
+            pltpu.VMEM((1, T), F32),
             pltpu.VMEM((16, 8, T), F32),
             pltpu.VMEM((NH, 2 * T, T), F32),
             pltpu.VMEM((NH // 2, T, T), F32),
@@ -485,10 +593,11 @@
             pltpu.VMEM((T, NH * HD), F32),
             pltpu.VMEM((4, T, T), F32),
             pltpu.VMEM((T, T), F32),
+            pltpu.VMEM((NH, 2 * T, T), BF16),
             pltpu.VMEM((NH, HD, T), F32),
             pltpu.VMEM((NH, HD, T), F32),
-            pltpu.VMEM((NH, HD, T), BF16),
-            pltpu.VMEM((NH, HD, T), BF16),
+            pltpu.VMEM((NH, HD // 2, T), BF16),
+            pltpu.VMEM((NH, HD // 2, T), BF16),
             pltpu.VMEM((NH // 2, T, T), F32),
             pltpu.VMEM((NH // 2, T, 2 * T), BF16),
             pltpu.VMEM((T, NH * HD), BF16),
@@ -516,7 +625,7 @@
             collective_id=0, has_side_effects=True, vmem_limit_bytes=60 * 1024 * 1024
         ),
         name="layer",
-    )(small, rate, hgain, egain, *big)
+    )(*args)
 
 
 def shards(
@@ -524,18 +633,10 @@
     head_gain, output_matrix, expert_gain, group_scores, expert_scores, routes,
     gate_weight, up_weight, down_weight,
 ):
-    small = jnp.concatenate(
-        [
-            write_logits[0], decay_logits[0], extra_decay[0], group_scores[0], expert_scores[0],
-            routes[0].astype(F32), jnp.zeros((T, T - 56), F32),
-        ],
-        axis=1,
-    )
-    rate = jnp.broadcast_to(head_rate[:, None], (8, T))
-    hgain = jnp.tile(head_gain, 2)[None]
     out = call(
-        small, rate, hgain, expert_gain[None], query[0], key[0], value[0], output_gate[0],
-        residual[0], output_matrix, gate_weight[0], up_weight[0], down_weight[0],
+        write_logits[0].T, decay_logits[0].T, extra_decay[0].T, group_scores[0].T, expert_scores[0].T,
+        routes[0].T, head_rate, head_gain[None], expert_gain[None], query[0], key[0], value[0],
+        output_gate[0], residual[0], output_matrix, gate_weight[0], up_weight[0], down_weight[0],
     )
     return out[None]
 

time: 106 us -> 88.6 us (0.84)
  Pallas kernels: 95.8 us -> 87 us
  local copies, waits for them, and re-layouts: 9.27 us -> 0.8 us
    pallas_call x1, Pallas kernels: 95.8 us -> 87 us  [call(): pl.pallas_call(kernel, out_shape=pltpu.VMEM((T, D), BF16), in_specs=[vm]...]
    unnamed x7 -> x1, local copies, waits for them, and re-layouts: 6.63 us -> 0.8 us
    another operation x2 -> x0, local copies, waits for them, and re-layouts: 1.24 us -> none  [shards(): hgain = jnp.tile(head_gain, 2)[None]]
where the time goes in v2:
time: 88.6 us; the launch traced here: 88.4 us
  Pallas kernels  87 us (98%)
    pallas_call x1, Pallas kernels, call(): pl.pallas_call(kernel, out_shape=pltpu.VMEM((T, D), BF16), in_specs=[vm]...  87 us

profile of v2, /device:TPU:1, one launch (start us, length us, event | category | flops | bytes accessed | tf_op | source)
XLA Modules:
  0.0 88.4 jit_solution(1092000565943797306)
XLA Ops:
  0.7 87.0 %layer.1 = bf16[128,2048]{1,0:T(8,128)(2,1)S(1)} custom-call(f32[16,128]{1,0:T(8,128)} %bitcast.38, f32[16,128]{1,0:T(8,128)} %bitcast.39, f32[16,128]{1,0:T(8,128)} %bitcast.40, f32[4,128]{1,0:T(4,128)} %bitcast.42, f32[2,128]{1,0:T(2,128)} %bitcast.43, s32[2,128]{1,0:T(2,128)} %bitcast.44, f32[1]{0:T(128)S(6)} %copy.21.rate_in, f32[1,64]{1,0:T(1,128)} %bitcast.45, ...), custom_call_target="tpu_custom_call" | custom-call | tf_op jit(solution)/shard_map/layer/pallas_call | solution.py:569
  87.6 0.8 copy.20

commit v3 on v2

--- a/solution.py
+++ b/solution.py
@@ -18,6 +18,7 @@
 NE = 128
 CHUNKS = 4
 PER = NE // CHUNKS
+OWN = 122
 
 
 def coords():
@@ -31,10 +32,10 @@
 
 
 def offset(i):
-    chunk = i >> 5
-    dx = (i >> 3) & 3
-    dy = (i >> 1) & 3
-    return (chunk - dx - dy) & 3, dx, dy, i & 1
+    chunk = 3 - (i >> 5)
+    dx = (i & 3) ^ 2
+    dy = ((i >> 2) & 3) ^ 2
+    return (chunk - dx - dy) & 3, dx, dy, 1 - ((i >> 4) & 1)
 
 
 def iota(shape, dim):
@@ -155,7 +156,8 @@
         dx = ((e >> 3) - x) & 3
         dy = ((e >> 1) - y) & 3
         dc = (e - c) & 1
-        return ((((dz + dx + dy) & 3) << 5) + (dx << 3) + (dy << 1) + dc) * 8 + rank
+        chunk = 3 - ((dz + dx + dy) & 3)
+        return ((chunk << 5) + ((1 - dc) << 4) + ((dy ^ 2) << 2) + (dx ^ 2)) * 8 + rank
 
     slot0 = slot_of(e0, rank0)
     slot1 = slot_of(e1, rank1)
@@ -275,19 +277,20 @@
     sub64 = iota((HD, T), 0)
 
     def heads(step, carry):
-        n = (z + 3 - step) & 3
-        col = cols.at[n]
+        base = 8 * (((z >> 1) + 1 - step) & 1)
         causal = sub >= lane
         ls, ups, ws, kds, tots = [], [], [], [], []
-        for hh in range(4):
-            h = n * 4 + hh
+        for hh in range(8):
+            h = base + hh
+            col = cols.at[h >> 2]
+            cc = hh % 4
             c_row = rows_ref[pl.ds(h, 1), :]
             k_row = rows_ref[pl.ds(h + 16, 1), :]
             b_row = rows_ref[pl.ds(h + 32, 1), :]
-            c_col = col[:, hh : hh + 1]
+            c_col = col[:, cc : cc + 1]
             dec = jnp.where(causal, jnp.exp(jnp.minimum(c_col - c_row, 0.0)), 0.0) * k_row
-            ls.append(jnp.where(sub > lane, raw[h, 0:T, :] * dec * col[:, hh + 16 : hh + 17], 0.0))
-            raw[h, T : 2 * T, :] = raw[h, T : 2 * T, :] * dec * col[:, hh + 32 : hh + 33]
+            ls.append(jnp.where(sub > lane, raw[h, 0:T, :] * dec * col[:, cc + 16 : cc + 17], 0.0))
+            raw[h, T : 2 * T, :] = raw[h, T : 2 * T, :] * dec * col[:, cc + 32 : cc + 33]
             ups.append(b_row)
             ws.append(b_row * k_row * jnp.exp(c_row))
             last = c_row[:, T - 1 : T]
@@ -315,8 +318,8 @@
             ys_ = [dot4(split(o), split(with_odd_blocks(none, x_, size))) for o, x_ in zip(odd, xs_)]
             ts = [with_odd_blocks(t, o - y_, size) for t, o, y_ in zip(ts, odd, ys_)]
         uws = []
-        for hh in range(4):
-            h = n * 4 + hh
+        for hh in range(8):
+            h = base + hh
             uh, ul = split(ts[hh] * ups[hh])
             wh, wl = split(ts[hh] * ws[hh])
             vm = rhs_v[h]
@@ -325,16 +328,16 @@
             uws.append(split(uw))
             uwbuf[h, 0:T, :] = uws[hh][0]
             uwbuf[h, T : 2 * T, :] = uws[hh][1]
-        for hh in range(4):
-            h = n * 4 + hh
-            ktp = kt_ref[n * 2 + hh // 2, (hh % 2) * HD : (hh % 2) * HD + HD, :]
+        for hh in range(8):
+            h = base + hh
+            ktp = kt_ref[h >> 1, (hh % 2) * HD : (hh % 2) * HD + HD, :]
             bn = dot4(split(ktp * kds[hh]), uws[hh])
             if hh % 2:
                 bn = roll64(bn)
             ident = jnp.where(lane64 - HD == sub64, tots[hh], 0.0)
             mb_out[h] = jnp.where(lane64 < HD, bn, ident - bn)
-        for hh in range(4):
-            h = n * 4 + hh
+        for hh in range(8):
+            h = base + hh
 
             @pl.when(h == sp)
             def _():
@@ -344,12 +347,12 @@
             def _():
                 pltpu.make_async_remote_copy(
                     mb_out.at[h], mb_in.at[sp], mb_sem.at[0], mb_sem.at[1],
-                    device_id=at(n, hh, y, c), device_id_type=MESH,
+                    device_id=at(h >> 2, hh, y, c), device_id_type=MESH,
                 ).start()
 
         return carry
 
-    lax.fori_loop(0, 4, heads, 0)
+    lax.fori_loop(0, 2, heads, 0)
 
     def inside(n, carry):
         col = cols.at[n]
@@ -473,7 +476,7 @@
             i = n * PER + j
             dz, dx, dy, dc = offset(i)
 
-            @pl.when(i != 0)
+            @pl.when(i != OWN)
             def _():
                 pltpu.make_async_remote_copy(
                     out_buf.at[i], arrived.at[i], fwd_send, fwd_recv.at[n],
@@ -486,7 +489,7 @@
         return carry
 
     lax.fori_loop(0, CHUNKS, dispatch, 0)
-    arrived[0] = out_buf[0]
+    arrived[OWN] = out_buf[OWN]
     loads[6].wait()
     loads[7].wait()
     loads[8].wait()
@@ -503,7 +506,7 @@
             i = n * PER + j
             dz, dx, dy, dc = offset(i)
 
-            @pl.when(i != 0)
+            @pl.when(i != OWN)
             def _():
                 pltpu.make_async_remote_copy(
                     prod.at[i], back.at[i], ret_send, ret_recv.at[n],
@@ -514,13 +517,17 @@
 
         lax.fori_loop(0, PER, send, 0)
     def expert(n, carry):
-        @pl.when(n == 0)
+        @pl.when(n == 3)
         def _():
-            many_recv(arrived, PER - 1, fwd_recv.at[0])
-
-        @pl.when(n != 0)
+            many_recv(arrived, PER - 1, fwd_recv.at[3])
+
+        @pl.when(n != 3)
         def _():
             many_recv(arrived, PER, fwd_recv.at[n])
+
+        @pl.when(n >= 1)
+        def _():
+            send_back(n - 1)
 
         rows = arrived[pl.ds(n * PER, PER)].reshape(256, HALF)
         xs[...] = dot(apart, rows).astype(BF16)
@@ -535,18 +542,14 @@
             xs[half * T : (half + 1) * T, inside] = dot(acc[...], wd_ref[:, cut]).astype(BF16)
         prod[pl.ds(n * PER, PER)] = dot(together, xs[...]).astype(BF16).reshape(PER, 8, HALF)
 
-        @pl.when(n >= 1)
-        def _():
-            send_back(n - 1)
-
         return carry
 
     lax.fori_loop(0, CHUNKS, expert, 0)
     send_back(3)
-    back[0] = prod[0]
+    back[OWN] = prod[OWN]
 
     for n in range(CHUNKS):
-        many_recv(back, PER - 1 if n == 0 else PER, ret_recv.at[n])
+        many_recv(back, PER - 1 if n == 3 else PER, ret_recv.at[n])
         part = dot(wsel[:, n * 256 : (n + 1) * 256], back[n * PER : (n + 1) * PER].reshape(256, HALF))
         for h in range(2):
             cut = slice(h * HALF, (h + 1) * HALF)

time: 88.6 us -> 84.3 us (0.951)
  Pallas kernels: 87 us -> 82.7 us
    pallas_call x1, Pallas kernels: 87 us -> 82.7 us  [call(): pl.pallas_call(kernel, out_shape=pltpu.VMEM((T, D), BF16), in_specs=[vm]...]
where the time goes in v3:
time: 84.3 us; the launch traced here: 84.1 us
  Pallas kernels  82.7 us (98%)
    pallas_call x1, Pallas kernels, call(): pl.pallas_call(kernel, out_shape=pltpu.VMEM((T, D), BF16), in_specs=[vm]...  82.7 us

profile of v3, /device:TPU:1, one launch (start us, length us, event | category | flops | bytes accessed | tf_op | source)
XLA Modules:
  0.0 84.1 jit_solution(9011688244787476154)
XLA Ops:
  0.7 82.7 %layer.1 = bf16[128,2048]{1,0:T(8,128)(2,1)S(1)} custom-call(f32[16,128]{1,0:T(8,128)} %bitcast.38, f32[16,128]{1,0:T(8,128)} %bitcast.39, f32[16,128]{1,0:T(8,128)} %bitcast.40, f32[4,128]{1,0:T(4,128)} %bitcast.42, f32[2,128]{1,0:T(2,128)} %bitcast.43, s32[2,128]{1,0:T(2,128)} %bitcast.44, f32[1]{0:T(128)S(6)} %copy.21.rate_in, f32[1,64]{1,0:T(1,128)} %bitcast.45, ...), custom_call_target="tpu_custom_call" | custom-call | tf_op jit(solution)/shard_map/layer/pallas_call | solution.py:572
  83.3 0.8 copy.20

commit v4 on v3

--- a/solution.py
+++ b/solution.py
@@ -18,6 +18,7 @@
 NE = 128
 CHUNKS = 4
 PER = NE // CHUNKS
+FAR = (10, 2, 8, 6, 14, 9, 11, 1, 3, 4, 12, 5, 7, 13, 15)
 OWN = 122
 
 
@@ -117,8 +118,10 @@
         pl.semaphore_signal(barrier, 1, device_id=at(z, x, y + (i >> 1), c + i), device_id_type=MESH)
         return carry
 
-    lax.fori_loop(1, 16, greet_sp, 0)
-    lax.fori_loop(1, 8, greet_dp, 0)
+    for i in FAR:
+        greet_sp(i, 0)
+    for i in range(1, 8):
+        greet_dp(i, 0)
 
     def many_recv(buf, count, sem):
         part = buf.at[pl.ds(0, count)]
@@ -235,13 +238,15 @@
         ).start()
         return carry
 
-    lax.fori_loop(1, 16, send_rate, 0)
+    for i in FAR:
+        send_rate(i, 0)
 
     def tell_in(i, carry):
         pl.semaphore_signal(all_in, 1, device_id=at(z, x, y + (i >> 1), c + i), device_id_type=MESH)
         return carry
 
-    lax.fori_loop(1, 8, tell_in, 0)
+    for i in range(1, 8):
+        tell_in(i, 0)
     rates[sp] = rate_ref[...]
     is_head = lane < NH
     beta = jax.nn.sigmoid(jnp.where(is_head, small, 0.0))
@@ -309,7 +314,7 @@
         tsp = [split(t) for t in ts]
         xsp = [split(dot3(split(jnp.where(m, l, 0.0)), t)) for l, t in zip(ls, tsp)]
         ts = [t - dot3(tp, xx) for t, tp, xx in zip(ts, tsp, xsp)]
-        for bits in range(3, 7):
+        for bits in range(3, 6):
             size = 1 << bits
             m = (lane64 >> bits) == 2 * (sub64 >> bits)
             none = jnp.zeros((T, T), F32)
@@ -317,6 +322,19 @@
             odd = [odd_blocks(t, size) for t in ts]
             ys_ = [dot4(split(o), split(with_odd_blocks(none, x_, size))) for o, x_ in zip(odd, xs_)]
             ts = [with_odd_blocks(t, o - y_, size) for t, o, y_ in zip(ts, odd, ys_)]
+        xs_ = []
+        for l, t in zip(ls, ts):
+            (lh, ll), (th, tl) = split(l[HD:]), split(t[:HD])
+            lh32, ll32 = lh.astype(F32), ll.astype(F32)
+            left = jnp.where(lane64 < HD, lh32, roll64(ll32)).astype(BF16)
+            xs_.append(dot(jnp.concatenate([left, left], axis=1), jnp.concatenate([th, th, tl, tl], axis=0)))
+        lowers = []
+        for t, x_ in zip(ts, xs_):
+            (th, tl), (xh, xl) = split(t[HD:]), split(x_)
+            left = jnp.where(lane64 < HD, roll64(tl.astype(F32)), th.astype(F32)).astype(BF16)
+            y_ = dot(jnp.concatenate([left, left], axis=1), jnp.concatenate([xh, xh, xl, xl], axis=0))
+            lowers.append(t[HD:] - y_)
+        ts = [jnp.concatenate([t[:HD], low], axis=0) for t, low in zip(ts, lowers)]
         uws = []
         for hh in range(8):
             h = base + hh
@@ -431,7 +449,8 @@
         ).start()
         return carry
 
-    lax.fori_loop(1, 16, send_state, 0)
+    for i in FAR:
+        send_state(i, 0)
     s_in[sp] = s_out[sp]
 
     many_recv(s_in, 15, s_sem.at[1])

time: 84.3 us -> 84.7 us (level)
  no operation moved by 1% of the time
where the time goes in v4:
time: 84.7 us; the launch traced here: 84.3 us
  Pallas kernels  82.8 us (98%)
    pallas_call x1, Pallas kernels, call(): pl.pallas_call(kernel, out_shape=pltpu.VMEM((T, D), BF16), in_specs=[vm]...  82.8 us

profile of v4, /device:TPU:1, one launch (start us, length us, event | category | flops | bytes accessed | tf_op | source)
XLA Modules:
  0.0 84.3 jit_solution(1460607325690885868)
XLA Ops:
  0.7 82.8 %layer.1 = bf16[128,2048]{1,0:T(8,128)(2,1)S(1)} custom-call(f32[16,128]{1,0:T(8,128)} %bitcast.38, f32[16,128]{1,0:T(8,128)} %bitcast.39, f32[16,128]{1,0:T(8,128)} %bitcast.40, f32[4,128]{1,0:T(4,128)} %bitcast.42, f32[2,128]{1,0:T(2,128)} %bitcast.43, s32[2,128]{1,0:T(2,128)} %bitcast.44, f32[1]{0:T(128)S(6)} %copy.21.rate_in, f32[1,64]{1,0:T(1,128)} %bitcast.45, ...), custom_call_target="tpu_custom_call" | custom-call | tf_op jit(solution)/shard_map/layer/pallas_call | solution.py:591
  83.5 0.8 copy.20
